TPU v7x, 32 devices: a whole 2x2x4 slice. The times are simulated.
32 devices in a mesh: sp: 4 (over y, x), tp: 8 (over z, core).
Axes of the slice: x: 2, y: 2, z: 4, core: 2. Of those that a mesh axis runs over, the one named last changes fastest.
Arguments:
- residual: bfloat16 [4096, 2048], P(('sp', 'tp')), may hold values from -6 to 6
- wide_query: bfloat16 [4096, 1024], P('sp', 'tp'), may hold values from -8 to 8
- narrow_query: bfloat16 [4096, 1024], P('sp', 'tp'), may hold values from -8 to 8
- wide_keys: bfloat16 [4096, 256], P('sp'), may hold values from -6 to 6
- narrow_keys: bfloat16 [4096, 256], P('sp'), may hold values from -6 to 6
- wide_values: bfloat16 [4096, 256], P('sp'), may hold values from -6 to 6
- narrow_values: bfloat16 [4096, 256], P('sp'), may hold values from -6 to 6
- wide_query_gain: float32 [64], replicated, may hold values from 1.2 to 10
- wide_key_gain: float32 [64], replicated, may hold values from 1.2 to 10
- narrow_query_gain: float32 [32], replicated, may hold values from 1.2 to 10
- narrow_key_gain: float32 [32], replicated, may hold values from 1.2 to 10
- wide_out: bfloat16 [1024, 2048], P('tp'), may hold values from -0.25 to 0.25
- narrow_out: bfloat16 [1024, 2048], P('tp'), may hold values from -0.25 to 0.25
- first_gain: float32 [2048], replicated, may hold values from 0.1 to 1.9
- first_bias: float32 [2048], replicated, may hold values from -1.8 to 1.8
- route_ids: int32 [4096, 2], P(('sp', 'tp')), may hold values from 0 to 7, all different within a row; in each aligned block of 128 rows (0 to 127, 128 to 255, ...) at most 40 rows name the same one
- route_weights: float32 [4096, 2], P(('sp', 'tp')), may hold values from 0.25 to 2.5
- expert_gate: bfloat16 [8, 2048, 3072], P('sp', None, 'tp'), may hold values from -0.125 to 0.125
- expert_up: bfloat16 [8, 2048, 3072], P('sp', None, 'tp'), may hold values from -0.125 to 0.125
- expert_down: bfloat16 [8, 3072, 2048], P('sp', 'tp'), may hold values from -0.109375 to 0.109375
- shared_gate: bfloat16 [2048, 256], replicated, may hold values from -0.125 to 0.125
- shared_up: bfloat16 [2048, 256], replicated, may hold values from -0.125 to 0.125
- shared_down: bfloat16 [256, 2048], replicated, may hold values from -0.375 to 0.375
- second_gain: float32 [2048], replicated, may hold values from 0.1 to 1.9
- second_bias: float32 [2048], replicated, may hold values from -1.8 to 1.8
Outputs:
- layer_output: bfloat16 [4096, 2048], P(('sp', 'tp'))
Inputs may be any that keep to these rules, and one draw needn't show every extreme that they name: `route_ids`: each row names 2 different experts. The rows of one device (aligned blocks of 128 rows) name each expert at most 40 times, and in every draw some expert is named exactly 40 times in the rows of some device.
All inputs are finite; a program needn't handle non-finite values.
Results may differ from a plain program's by a relative error of at most 0.02.
The roundings to bfloat16 on the way count: a program that leaves them out, or rounds other values in their place, can miss the bound.
Values may be sent and summed in bfloat16 or wider, within the bound.
A program may use at most 128 MiB of HBM per device.

v0:
```python
import functools
import math

import jax
import jax.numpy as jnp
import numpy as np
from jax import lax
from jax.experimental import pallas as pl
from jax.experimental.pallas import tpu as pltpu
from jax.sharding import PartitionSpec as P

WIDE_HEADS = 16
WIDE_GROUPS = 4
NARROW_HEADS = 32
NARROW_GROUPS = 8
GRID_WIDTH = 64
SEQ_SHARDS = 4
LOCAL_EXPERTS = 2


EPS_HEAD = 1e-06
EPS_LAYER = 1e-05
ALPHA = 2.0**0.25
THETA = 10000.0


def line_order(place, count, step):
    mirrored = place >= (count + 1) // 2
    near = jnp.where(mirrored, count - 1 - place, place)
    swing = jnp.where(step % 2 == 1, near + (step + 1) // 2, near - step // 2)
    spot = jnp.where(step <= 2 * near, swing, step)
    return jnp.where(mirrored, count - 1 - spot, spot)


def angle_tables(head_size, lanes, grid_rows):
    half, quarter = head_size // 2, head_size // 4
    lane = np.arange(lanes)
    spot = lane % half
    frequency = THETA ** (-(spot % quarter) / quarter)
    by_row = lane % head_size < half
    sign = np.where(spot < quarter, -1.0, 1.0)
    angles = np.arange(max(grid_rows, GRID_WIDTH))[:, None] * frequency[None, :]
    tables = []
    for keep, count in ((by_row, grid_rows), (~by_row, GRID_WIDTH)):
        tables.append(np.where(keep, np.cos(angles[:count]), 0.0))
        tables.append(np.where(keep, sign * np.sin(angles[:count]), 0.0))
    return [table.astype(np.float32) for table in tables]


def attention_kernel(
    wide_query,
    narrow_query,
    wide_keys,
    narrow_keys,
    wide_values,
    narrow_values,
    gains,
    wide_row_cos,
    wide_row_sin,
    wide_col_cos,
    wide_col_sin,
    narrow_row_cos,
    narrow_row_sin,
    narrow_col_cos,
    narrow_col_sin,
    residual,
    wide_out,
    narrow_out,
    norm_gain,
    norm_bias,
    hidden_ref,
    wide_kv,
    narrow_kv,
    values_ones,
    wide_heads,
    narrow_heads,
    out_all,
    mixed,
    gathered,
    projected,
    load_sem,
    kv_send,
    kv_recv,
    kv_pair_send,
    kv_pair_recv,
    line_send,
    line_recv,
    out_pair_send,
    out_pair_recv,
    share_send,
    share_recv,
    mixed_send,
    mixed_recv,
    *,
    tp_size,
    shards,
    wide_size,
    narrow_size,
    local_wide,
    local_narrow,
):
    n_z = tp_size // 2
    lanes = 128
    tokens, width = residual.shape
    seg_rows = wide_query.shape[0]
    half_rows = seg_rows // 2
    prep_rows = 256
    prep_grid = prep_rows // GRID_WIDTH
    out_rows = wide_out.shape[0]
    piece = 2 * out_rows // shards
    me_sp = lax.axis_index("sp")
    me_tp = lax.axis_index("tp")
    z = me_tp // 2
    core = me_tp % 2
    peer = me_tp + 1 - 2 * core
    shard = me_sp % shards
    first_sp = me_sp - shard
    kinds = (wide_kv, narrow_kv)

    def remote(src, dst, send_sem, recv_sem, sp, tp):
        return pltpu.make_async_remote_copy(
            src_ref=src,
            dst_ref=dst,
            send_sem=send_sem,
            recv_sem=recv_sem,
            device_id=(sp, tp),
            device_id_type=pl.DeviceIdType.MESH,
        )

    def kv_part(kind, owner, side):
        start = pl.multiple_of(owner * seg_rows + side * half_rows, half_rows)
        return kinds[kind].at[pl.ds(start, half_rows)]

    def kv_copy(kind, j):
        part = kv_part(kind, shard, core)
        return remote(
            part, part, kv_send.at[kind, j], kv_recv.at[kind, j], first_sp + (shard + j) % shards, me_tp
        )

    def kv_pair(kind, j):
        part = kv_part(kind, (shard - j + shards) % shards, core)
        return remote(
            part, part, kv_pair_send.at[kind, j], kv_pair_recv.at[kind, j], me_sp, peer
        )

    def out_piece(place, owner):
        return out_all.at[2 * place + core, pl.ds(pl.multiple_of(owner * piece, piece), piece)]

    def line_copy(way, d):
        part = out_piece(z, shard)
        return remote(
            part, part, line_send.at[way, d], line_recv.at[z], me_sp, me_tp + (2 - 4 * way) * d
        )

    def out_pair(place, j):
        part = out_piece(place, (shard - j + shards) % shards)
        return remote(part, part, out_pair_send.at[place, j], out_pair_recv.at[place, j], me_sp, peer)

    def own_pair():
        part = out_all.at[me_tp]
        return remote(part, part, out_pair_send.at[z, 0], out_pair_recv.at[z, 0], me_sp, peer)

    def share_copy(place, j):
        part = out_piece(place, shard)
        return remote(
            part, part, share_send.at[place, j], share_recv.at[place, j],
            first_sp + (shard + j) % shards, me_tp,
        )

    def mixed_copy(kind, b):
        target = (me_tp + 1 + b) % tp_size
        return remote(
            mixed.at[kind, target],
            gathered.at[me_tp, :, pl.ds(kind * lanes, lanes)],
            mixed_send.at[kind, b],
            mixed_recv.at[kind, b],
            me_sp,
            target,
        )

    loads = [
        pltpu.make_async_copy(
            src, out_all.at[me_tp, pl.ds(i * out_rows, out_rows)], load_sem.at[i]
        )
        for i, src in enumerate((wide_out, narrow_out))
    ]
    for copy in loads:
        copy.start()

    lane = lax.broadcasted_iota(jnp.int32, (1, lanes), 1)

    def normalized(values, size, gain_row, row_cos, row_sin, col_cos, col_sin, i):
        squares = values * values
        high = squares.astype(jnp.bfloat16)
        low = (squares - high.astype(jnp.float32)).astype(jnp.bfloat16)
        left = lax.broadcasted_iota(jnp.int32, (lanes, lanes), 0) // size
        right = lax.broadcasted_iota(jnp.int32, (lanes, lanes), 1) // size
        same = jnp.where(left == right, 1.0, 0.0).astype(jnp.bfloat16)
        total = jnp.dot(high, same, preferred_element_type=jnp.float32) + jnp.dot(
            low, same, preferred_element_type=jnp.float32
        )
        scaled = values * lax.rsqrt(total * (1.0 / size) + EPS_HEAD) * gains[gain_row : gain_row + 1, :]
        quarter = size // 4
        partner = jnp.where(
            lane % (size // 2) < quarter,
            pltpu.roll(scaled, lanes - quarter, 1),
            pltpu.roll(scaled, quarter, 1),
        )
        grid_row = (shard * (seg_rows // prep_rows) + i) * prep_grid

        def spread(by_row, by_col):
            lines = by_row[pl.ds(grid_row, prep_grid), :]
            return jnp.concatenate([lines[g : g + 1, :] + by_col[...] for g in range(prep_grid)], axis=0)

        return scaled * spread(row_cos, col_cos) + partner * spread(row_sin, col_sin)

    wide_tables = (wide_row_cos, wide_row_sin, wide_col_cos, wide_col_sin)
    narrow_tables = (narrow_row_cos, narrow_row_sin, narrow_col_cos, narrow_col_sin)

    def column_pick(source, group, size):
        column = lax.broadcasted_iota(jnp.int32, (source.shape[1], lanes), 0)
        return jnp.where(column == group * size + lane % size, 1.0, 0.0).astype(jnp.bfloat16)

    def key_step(kind, i, keys, values, picks, size, gain_row, tables):
        rows = pl.ds(pl.multiple_of(i * prep_rows, prep_rows), prep_rows)
        own_keys = jnp.dot(keys[rows, :], picks, preferred_element_type=jnp.float32)
        own_values = jnp.dot(values[rows, :], picks, preferred_element_type=jnp.float32)
        rotated = normalized(own_keys, size, gain_row, *tables, i)
        packed = jnp.where((lane // size) % 2 == 0, rotated, own_values).astype(jnp.bfloat16)
        start = pl.multiple_of(shard * seg_rows + i * prep_rows, prep_rows)
        kinds[kind][pl.ds(start, prep_rows), :] = packed

    per_wide = WIDE_HEADS // WIDE_GROUPS
    per_narrow = NARROW_HEADS // NARROW_GROUPS
    wide_picks = column_pick(wide_keys, me_tp * local_wide // per_wide, wide_size)
    lower_group = 2 * z * local_narrow // per_narrow
    upper_group = (2 * z + 1) * local_narrow // per_narrow
    narrow_picks = column_pick(
        narrow_keys, jnp.where(lane < lanes // 2, lower_group, upper_group), narrow_size
    )
    blocks = seg_rows // prep_rows

    @pl.loop(0, blocks)
    def _(i):
        key_step(0, i, wide_keys, wide_values, wide_picks, wide_size, 1, wide_tables)

    for j in range(1, shards):
        kv_copy(0, j).start()

    for copy in loads:
        copy.wait()
    own_pair().start()

    for d in range(1, n_z):

        @pl.when(z + d < n_z)
        def _():
            line_copy(0, d).start()

        @pl.when(z - d >= 0)
        def _():
            line_copy(1, d).start()

    @pl.loop(0, blocks)
    def _(i):
        key_step(1, i, narrow_keys, narrow_values, narrow_picks, narrow_size, 3, narrow_tables)

    for j in range(1, shards):
        kv_copy(1, j).start()
    @pl.loop(0, blocks)
    def _(i):
        rows = pl.ds(pl.multiple_of(i * prep_rows, prep_rows), prep_rows)
        rotated = normalized(
            wide_query[rows, :].astype(jnp.float32), wide_size, 0, *wide_tables, i
        )
        for h in range(local_wide):
            moved = rotated if h == 0 else pltpu.roll(rotated, lanes - h * wide_size, 1)
            wide_heads[h, rows] = jnp.where(lane < wide_size, moved, 0.0).astype(jnp.bfloat16)
        rotated = normalized(
            narrow_query[rows, :].astype(jnp.float32), narrow_size, 2, *narrow_tables, i
        )
        for h in range(local_narrow):
            shift = (core * (lanes // 2) + lanes - h * narrow_size) % lanes
            moved = pltpu.roll(rotated, shift, 1)
            kept = lane // narrow_size == 2 * core
            narrow_heads[h, rows] = jnp.where(kept, moved, 0.0).astype(jnp.bfloat16)

    def attend(block, kv, size):
        scores = lax.dot_general(
            block, kv[...], (((1,), (1,)), ((), ())), preferred_element_type=jnp.float32
        )
        largest = jnp.max(scores, axis=-1, keepdims=True)
        factor = math.log2(math.e) * size ** (-0.5)
        weights = jnp.exp2((scores - largest) * factor).astype(jnp.bfloat16)
        sums = jnp.dot(weights, values_ones[...], preferred_element_type=jnp.float32)
        return sums / sums[:, 0:1]

    def relay_kv(kind):
        for j in range(1, shards):
            kv_copy(kind, j).wait_recv()
            kv_pair(kind, j).start()
        for j in range(1, shards):
            kv_pair(kind, j).wait_recv()
        size = (wide_size, narrow_size)[kind]
        keep = jnp.where((lane // size) % 2 == 1, 1.0, 0.0).astype(jnp.bfloat16)
        fill = jnp.where((lane // size) % 2 == 1, 0.0, 1.0).astype(jnp.bfloat16)

        @pl.loop(0, shards * blocks)
        def _(i):
            rows = pl.ds(pl.multiple_of(i * prep_rows, prep_rows), prep_rows)
            values_ones[rows, :] = kinds[kind][rows, :] * keep + fill

    def put_mixed(kind, b, target, value):
        @pl.when(b < tp_size - 1)
        def _():
            mixed[kind, target] = value
            mixed_copy(kind, b).start()

        @pl.when(b == tp_size - 1)
        def _():
            gathered[target, :, kind * lanes : (kind + 1) * lanes] = value

    def share_step(step):
        place = line_order(z, n_z, step)
        part = out_piece(place, shard)
        pltpu.make_async_copy(part, part, line_recv.at[place]).wait()
        for j in range(1, shards):
            share_copy(place, j).start()
        out_pair(place, 0).start()

    early = (tp_size - tp_size // 2 + 2) // 3
    relay_kv(0)

    @pl.loop(0, tp_size)
    def _(b):
        @pl.when(jnp.logical_and(b >= tp_size // 2, (b - tp_size // 2) % 3 == 0))
        def _():
            share_step((b - tp_size // 2) // 3 + 1)

        target = (me_tp + 1 + b) % tp_size
        rows = pl.ds(pl.multiple_of(target * tokens, tokens), tokens)
        block = jnp.concatenate([wide_heads[h, rows] for h in range(local_wide)], axis=0)
        values = attend(block, wide_kv, wide_size)
        total = jnp.zeros((tokens, lanes), jnp.float32)
        for h in range(local_wide):
            part = values[h * tokens : (h + 1) * tokens]
            shift = ((h + 1) * wide_size) % lanes
            moved = part if shift == 0 else pltpu.roll(part, shift, 1)
            total = total + jnp.where(lane // wide_size == h, moved, 0.0)
        put_mixed(0, b, target, total.astype(jnp.bfloat16))

    relay_kv(1)

    @pl.loop(0, tp_size)
    def _(b):
        @pl.when(jnp.logical_and(b > 0, b + early < n_z))
        def _():
            share_step(b + early)

        @pl.when(b > tp_size - n_z)
        def _():
            place = line_order(z, n_z, b - (tp_size - n_z))
            for j in range(1, shards):
                share_copy(place, j).wait_recv()
                out_pair(place, j).start()

        target = (me_tp + 1 + b) % tp_size
        rows = pl.ds(pl.multiple_of(target * tokens, tokens), tokens)
        total = jnp.zeros((tokens, lanes), jnp.float32)
        for first in range(0, local_narrow, 2):
            block = jnp.concatenate([narrow_heads[first + h, rows] for h in range(2)], axis=0)
            values = attend(block, narrow_kv, narrow_size)
            for h in range(2):
                part = values[h * tokens : (h + 1) * tokens]
                shift = (
                    (first + h) * narrow_size + 2 * lanes - core * (lanes // 2) - narrow_size
                ) % lanes
                moved = pltpu.roll(part, shift, 1)
                total = total + jnp.where(lane // narrow_size == first + h, moved, 0.0)
        put_mixed(1, b, target, total.astype(jnp.bfloat16))

    @pl.loop(0, n_z)
    def _(place):
        @pl.when(place == z)
        def _():
            own_pair().wait_recv()

        @pl.when(place != z)
        def _():
            for j in range(shards):
                out_pair(place, j).wait_recv()

    @pl.loop(0, tp_size - 1)
    def _(b):
        mixed_copy(0, b).wait_recv()
        mixed_copy(1, b).wait_recv()

    chunk = 512
    for start in range(0, width, chunk):

        def add(q, total):
            if out_rows == lanes:
                return total + jnp.dot(
                    gathered[q],
                    out_all[q, :, start : start + chunk],
                    preferred_element_type=jnp.float32,
                )
            for kind in range(2):
                total = total + jnp.dot(
                    gathered[q, :, kind * lanes : kind * lanes + out_rows],
                    out_all[q, kind * out_rows : (kind + 1) * out_rows, start : start + chunk],
                    preferred_element_type=jnp.float32,
                )
            return total

        projected[:, start : start + chunk] = lax.fori_loop(
            0, tp_size, add, ALPHA * residual[:, start : start + chunk].astype(jnp.float32)
        )

    values = projected[...]
    center = jnp.mean(values, axis=-1, keepdims=True)
    shifted = values - center
    variance = jnp.mean(shifted * shifted, axis=-1, keepdims=True)
    hidden_ref[...] = (
        shifted * lax.rsqrt(variance + EPS_LAYER) * norm_gain[...] + norm_bias[...]
    ).astype(jnp.bfloat16)

    own_pair().wait_send()
    for j in range(1, shards):
        for kind in range(2):
            kv_copy(kind, j).wait_send()
            kv_pair(kind, j).wait_send()

    @pl.loop(0, n_z)
    def _(place):
        @pl.when(jnp.logical_and(place > 0, z + place < n_z))
        def _():
            line_copy(0, place).wait_send()

        @pl.when(jnp.logical_and(place > 0, z - place >= 0))
        def _():
            line_copy(1, place).wait_send()

        @pl.when(place != z)
        def _():
            for j in range(shards):
                out_pair(place, j).wait_send()
            for j in range(1, shards):
                share_copy(place, j).wait_send()

    @pl.loop(0, tp_size - 1)
    def _(b):
        mixed_copy(0, b).wait_send()
        mixed_copy(1, b).wait_send()


def attention(
    queries, keys_values, gain_vecs, residual, wide_out, narrow_out, first_gain, first_bias
):
    tp_size = lax.axis_size("tp")
    n_z = tp_size // 2
    lanes = 128
    tokens, width = residual.shape
    seg_rows = queries[0].shape[0]
    shards = SEQ_SHARDS
    sizes = gain_vecs[0].shape[0], gain_vecs[2].shape[0]
    local_heads = [q.shape[1] // size for q, size in zip(queries, sizes)]
    queries = [jnp.pad(q, ((0, 0), (0, lanes - q.shape[1]))) for q in queries]
    gains = jnp.concatenate(
        [gain for gain in gain_vecs for _ in range(lanes // gain.shape[0])]
    ).reshape(len(gain_vecs), lanes)
    grid_rows = shards * seg_rows // GRID_WIDTH
    tables = [
        jnp.asarray(table)
        for size in sizes
        for table in angle_tables(size, lanes, grid_rows)
    ]
    bf16 = jnp.bfloat16
    dma = pltpu.SemaphoreType.DMA
    vmem = pl.BlockSpec(memory_space=pltpu.VMEM)
    hbm = pl.BlockSpec(memory_space=pl.ANY)
    return pl.pallas_call(
        functools.partial(
            attention_kernel,
            tp_size=tp_size,
            shards=shards,
            wide_size=sizes[0],
            narrow_size=sizes[1],
            local_wide=local_heads[0],
            local_narrow=local_heads[1],
        ),
        out_shape=jax.ShapeDtypeStruct((tokens, width), bf16),
        in_specs=[vmem] * 16 + [hbm] * 2 + [vmem] * 2,
        out_specs=vmem,
        scratch_shapes=[
            pltpu.VMEM((shards * seg_rows, lanes), bf16),
            pltpu.VMEM((shards * seg_rows, lanes), bf16),
            pltpu.VMEM((shards * seg_rows, lanes), bf16),
            pltpu.VMEM((local_heads[0], seg_rows, lanes), bf16),
            pltpu.VMEM((local_heads[1], seg_rows, lanes), bf16),
            pltpu.VMEM((tp_size, 2 * wide_out.shape[0], width), bf16),
            pltpu.VMEM((2, tp_size, tokens, lanes), bf16),
            pltpu.VMEM((tp_size, tokens, 2 * lanes), bf16),
            pltpu.VMEM((tokens, width), jnp.float32),
            dma((2,)),
            dma((2, shards)),
            dma((2, shards)),
            dma((2, shards)),
            dma((2, shards)),
            dma((2, n_z)),
            dma((n_z,)),
            dma((n_z, shards)),
            dma((n_z, shards)),
            dma((n_z, shards)),
            dma((n_z, shards)),
            dma((2, tp_size)),
            dma((2, tp_size)),
        ],
        compiler_params=pltpu.CompilerParams(
            has_side_effects=True, vmem_limit_bytes=66_000_000
        ),
    )(
        *queries,
        *keys_values,
        gains,
        *tables,
        residual,
        wide_out,
        narrow_out,
        first_gain.reshape(1, width),
        first_bias.reshape(1, width),
    )


def moe_kernel(
    hidden_ref,
    meta_ref,
    shared_gate,
    shared_up,
    shared_down,
    norm_gain,
    norm_bias,
    gate_hbm,
    up_hbm,
    down_hbm,
    out_ref,
    gate_ref,
    up_ref,
    down_ref,
    hid,
    meta_all,
    rows,
    stage,
    act,
    peer_part,
    ret,
    own_half,
    result,
    spots_all,
    cross_send,
    cross,
    line_in,
    weight_sem,
    z_send,
    z_recv,
    pair_send,
    pair_recv,
    meta_send,
    meta_recv,
    x_send,
    x_recv,
    rows_send,
    rows_recv,
    part_send,
    part_recv,
    ret_send,
    ret_recv,
    cross_send_sem,
    cross_recv,
    line_send,
    line_recv,
    *,
    n_sp,
    tp_size,
    cap,
    slots,
):
    n_z = tp_size // 2
    tokens, width = hidden_ref.shape
    all_slots = n_sp * slots
    chunk = 512
    expert_lines = (LOCAL_EXPERTS * n_sp + 15) // 16 * 16
    me_sp = lax.axis_index("sp")
    me_tp = lax.axis_index("tp")
    z = me_tp // 2
    core = me_tp % 2
    peer = me_tp + 1 - 2 * core

    def remote(src, dst, send_sem, recv_sem, sp, tp):
        return pltpu.make_async_remote_copy(
            src_ref=src,
            dst_ref=dst,
            send_sem=send_sem,
            recv_sem=recv_sem,
            device_id=(sp, tp),
            device_id_type=pl.DeviceIdType.MESH,
        )

    weight_copies = [
        pltpu.make_async_copy(src, dst, weight_sem.at[i])
        for i, (src, dst) in enumerate(
            ((gate_hbm, gate_ref), (up_hbm, up_ref), (down_hbm, down_ref))
        )
    ]

    def line_copy(src, way, place):
        return remote(
            src,
            hid.at[place, core],
            z_send.at[way, place],
            z_recv.at[place],
            me_sp,
            me_tp + 2 - 4 * way,
        )

    def pair_copy(src, place):
        return remote(
            src, hid.at[place, core], pair_send.at[place], pair_recv.at[place], me_sp, peer
        )

    def meta_copy(j):
        return remote(
            meta_ref,
            meta_all.at[me_tp],
            meta_send.at[j],
            meta_recv.at[j],
            me_sp,
            (me_tp + j) % tp_size,
        )

    def slot_rows(sp):
        return pl.ds(pl.multiple_of(sp * slots, slots), slots)

    def x_copy(place, j):
        sp = (me_sp + j) % n_sp
        return remote(
            stage.at[place, slot_rows(sp)],
            rows.at[place, core, slot_rows(me_sp)],
            x_send.at[place, j],
            x_recv.at[place, j],
            sp,
            me_tp,
        )

    def rows_copy(place):
        return remote(
            rows.at[place, core],
            rows.at[place, core],
            rows_send.at[place],
            rows_recv.at[place],
            me_sp,
            peer,
        )

    def part_copy(place):
        return remote(
            rows.at[place, 1 - core],
            peer_part.at[place],
            part_send.at[place],
            part_recv.at[place],
            me_sp,
            peer,
        )

    def ret_copy(place, j):
        sp = (me_sp + j) % n_sp
        return remote(
            rows.at[place, core, slot_rows(sp)],
            ret.at[place, slot_rows(me_sp)],
            ret_send.at[place, j],
            ret_recv.at[place, j],
            sp,
            me_tp,
        )

    def cross_copy(place):
        return remote(
            cross_send.at[place],
            cross.at[place],
            cross_send_sem.at[place],
            cross_recv.at[place],
            me_sp,
            peer,
        )

    def line_up(place):
        return remote(
            cross.at[place], line_in.at[place], line_send.at[place], line_recv.at[place], me_sp, me_tp + 2
        )

    def line_dn(place):
        spot = jnp.where(place == z - 1, n_z, place)
        return remote(
            cross.at[place], line_in.at[spot], line_send.at[place], line_recv.at[spot], me_sp, me_tp - 2
        )

    pair_copy(hidden_ref, z).start()

    @pl.when(z < n_z - 1)
    def _():
        line_copy(hidden_ref, 0, z).start()

    @pl.when(z > 0)
    def _():
        line_copy(hidden_ref, 1, z).start()

    @pl.loop(1, tp_size)
    def _(j):
        meta_copy(j).start()

    for copy in weight_copies:
        copy.start()
    hid[z, core] = hidden_ref[...]
    meta_all[me_tp] = meta_ref[...]

    def selection(place, sp, weighted):
        expert = (LOCAL_EXPERTS * sp + core).astype(jnp.float32)
        parts = []
        for lane in range(2):
            info = meta_all[2 * place + lane]
            line = lax.broadcasted_iota(jnp.int32, (slots, tokens), 0).astype(jnp.float32)
            part = jnp.zeros((slots, tokens), jnp.float32)
            for choice in range(2):
                ids = info[choice : choice + 1, :tokens]
                spots = spots_all[2 * place + lane, choice : choice + 1, :tokens] + lane * cap
                target = jnp.where(ids == expert, spots, -1.0)
                value = info[2 + choice : 3 + choice, :tokens] if weighted else 1.0
                part = part + jnp.where(line == target, value, 0.0)
            parts.append(part)
        return jnp.concatenate(parts, axis=1)

    def shared_expert():
        gate_values = jnp.dot(hidden_ref[...], shared_gate[...], preferred_element_type=jnp.float32)
        up_values = jnp.dot(hidden_ref[...], shared_up[...], preferred_element_type=jnp.float32)
        active = (jax.nn.silu(gate_values) * up_values).astype(jnp.bfloat16)
        for start in range(0, width, chunk):
            cols = slice(start, start + chunk)
            result[:, cols] = ALPHA * hidden_ref[:, cols].astype(jnp.float32) + jnp.dot(
                active, shared_down[:, cols], preferred_element_type=jnp.float32
            )

    def send_step(step):
        place = line_order(z, n_z, step)

        @pl.when(step > 0)
        def _():
            pltpu.make_async_copy(hidden_ref, hid.at[place, core], z_recv.at[place]).wait()

            @pl.when(jnp.logical_and(place < z, z < n_z - 1))
            def _():
                line_copy(hid.at[place, core], 0, place).start()

            @pl.when(jnp.logical_and(place > z, z > 0))
            def _():
                line_copy(hid.at[place, core], 1, place).start()

            pair_copy(hid.at[place, core], place).start()

        pltpu.make_async_copy(hidden_ref, hid.at[place, 1 - core], pair_recv.at[place]).wait()
        for lane in range(2):
            j = (me_tp - 2 * place - lane + tp_size) % tp_size

            @pl.when(j > 0)
            def _():
                pltpu.make_async_copy(meta_ref, meta_all.at[2 * place + lane], meta_recv.at[j]).wait()

            info = meta_all[2 * place + lane]
            line = lax.broadcasted_iota(jnp.int32, (expert_lines, 128), 0).astype(jnp.float32)
            first = jnp.where(line == info[0:1, :], 1.0, 0.0)
            second = jnp.where(line == info[1:2, :], 1.0, 0.0)
            before = lax.broadcasted_iota(jnp.int32, (128, 128), 0) < lax.broadcasted_iota(
                jnp.int32, (128, 128), 1
            )
            counts = jnp.dot(
                (first + second).astype(jnp.bfloat16),
                jnp.where(before, 1.0, 0.0).astype(jnp.bfloat16),
                preferred_element_type=jnp.float32,
            )
            spots_all[2 * place + lane, 0:1] = jnp.sum(first * counts, axis=0, keepdims=True)
            spots_all[2 * place + lane, 1:2] = jnp.sum(second * counts, axis=0, keepdims=True)

        @pl.loop(0, n_sp)
        def _(i):
            j = (i + 1) % n_sp
            sp = (me_sp + j) % n_sp
            picks = selection(place, sp, False).astype(jnp.bfloat16)
            for start in range(0, width, chunk):
                piece = (
                    jnp.dot(
                        picks[:, :tokens],
                        hid[place, 0, :, start : start + chunk],
                        preferred_element_type=jnp.float32,
                    )
                    + jnp.dot(
                        picks[:, tokens:],
                        hid[place, 1, :, start : start + chunk],
                        preferred_element_type=jnp.float32,
                    )
                ).astype(jnp.bfloat16)
                stage[place, slot_rows(sp), start : start + chunk] = piece

            @pl.when(j > 0)
            def _():
                x_copy(place, j).start()

            @pl.when(j == 0)
            def _():
                rows[place, core, slot_rows(me_sp)] = stage[place, slot_rows(me_sp)]

    def compute_step(step):
        place = line_order(z, n_z, step)

        @pl.loop(1, n_sp)
        def _(j):
            x_copy(place, j).wait_recv()

        rows_copy(place).start()

        def expert(e):
            block = rows[place, e]
            gate_values = jnp.dot(block, gate_ref[e], preferred_element_type=jnp.float32)
            up_values = jnp.dot(block, up_ref[e], preferred_element_type=jnp.float32)
            act[...] = (jax.nn.silu(gate_values) * up_values).astype(jnp.bfloat16)

        def finish(e):
            for start in range(0, width, chunk):
                rows[place, e, :, start : start + chunk] = jnp.dot(
                    act[...], down_ref[e, :, start : start + chunk], preferred_element_type=jnp.float32
                ).astype(jnp.bfloat16)

        expert(core)
        rows_copy(place).wait()
        finish(core)
        expert(1 - core)
        finish(1 - core)
        part_copy(place).start()

    lag = 2

    @pl.loop(0, n_z + lag)
    def _(step):
        @pl.when(step < n_z)
        def _():
            send_step(step)

        @pl.when(step == 0)
        def _():
            shared_expert()

        @pl.when(step == lag)
        def _():
            for copy in weight_copies:
                copy.wait()

        @pl.when(step >= lag)
        def _():
            compute_step(step - lag)

    def return_step(step):
        place = line_order(z, n_z, n_z - 1 - step)
        part_copy(place).wait_recv()

        @pl.loop(0, n_sp)
        def _(i):
            j = (i + 1) % n_sp
            sp = (me_sp + j) % n_sp
            total = (
                rows[place, core, slot_rows(sp)].astype(jnp.float32)
                + peer_part[place, slot_rows(sp)].astype(jnp.float32)
            ).astype(jnp.bfloat16)

            @pl.when(j > 0)
            def _():
                rows[place, core, slot_rows(sp)] = total
                ret_copy(place, j).start()

            @pl.when(j == 0)
            def _():
                ret[place, slot_rows(me_sp)] = total

    def combine_step(step):
        place = line_order(z, n_z, n_z - 1 - step)

        @pl.loop(1, n_sp)
        def _(j):
            ret_copy(place, j).wait_recv()

        for lane in range(2):
            info = meta_all[2 * place + lane]
            lines = lax.broadcasted_iota(jnp.int32, (all_slots, tokens), 0).astype(jnp.float32)
            picks = jnp.zeros((all_slots, tokens), jnp.float32)
            for choice in range(2):
                ids = info[choice : choice + 1, :tokens]
                spots = spots_all[2 * place + lane, choice : choice + 1, :tokens] + lane * cap
                shard = jnp.floor(ids * 0.5)
                target = jnp.where(
                    ids - 2.0 * shard == core.astype(jnp.float32), shard * slots + spots, -1.0
                )
                picks = picks + jnp.where(
                    lines == target, info[2 + choice : 3 + choice, :tokens], 0.0
                )
            high = picks.astype(jnp.bfloat16)
            low = (picks - high.astype(jnp.float32)).astype(jnp.bfloat16)

            for start in range(0, width, chunk):
                piece = sum(
                    lax.dot_general(
                        part,
                        ret[place, :, start : start + chunk],
                        (((0,), (0,)), ((), ())),
                        preferred_element_type=jnp.float32,
                    )
                    for part in (high, low)
                )

                @pl.when(core == lane)
                def _():
                    own_half[:, start : start + chunk] = piece

                @pl.when(core != lane)
                def _():
                    cross_send[place, :, start : start + chunk] = piece.astype(jnp.bfloat16)

        cross_copy(place).start()
        cross_copy(place).wait_recv()
        own_half[...] = own_half[...] + cross[place].astype(jnp.float32)

        @pl.when(jnp.logical_and(z > 0, place >= z))
        def _():
            pltpu.make_async_copy(hidden_ref, line_in.at[place], line_recv.at[place]).wait()
            own_half[...] = own_half[...] + line_in[place].astype(jnp.float32)

        @pl.when(jnp.logical_and(z < n_z - 1, place <= z))
        def _():
            spot = jnp.where(place == z, n_z, place)
            pltpu.make_async_copy(hidden_ref, line_in.at[spot], line_recv.at[spot]).wait()
            own_half[...] = own_half[...] + line_in[spot].astype(jnp.float32)

        @pl.when(place == z)
        def _():
            values = own_half[...] + result[...]
            center = jnp.mean(values, axis=-1, keepdims=True)
            shifted = values - center
            variance = jnp.mean(shifted * shifted, axis=-1, keepdims=True)
            out_ref[...] = (
                shifted * lax.rsqrt(variance + EPS_LAYER) * norm_gain[...] + norm_bias[...]
            ).astype(jnp.bfloat16)

        @pl.when(place > z)
        def _():
            cross[place] = own_half[...].astype(jnp.bfloat16)
            line_up(place).start()

        @pl.when(place < z)
        def _():
            cross[place] = own_half[...].astype(jnp.bfloat16)
            line_dn(place).start()

    @pl.loop(0, n_z + 1)
    def _(step):
        @pl.when(step < n_z)
        def _():
            return_step(step)

        @pl.when(step > 0)
        def _():
            combine_step(step - 1)

    @pl.loop(0, n_z)
    def _(place):
        pair_copy(hidden_ref, place).wait_send()

        @pl.when(jnp.logical_and(place <= z, z < n_z - 1))
        def _():
            line_copy(hidden_ref, 0, place).wait_send()

        @pl.when(jnp.logical_and(place >= z, z > 0))
        def _():
            line_copy(hidden_ref, 1, place).wait_send()

        part_copy(place).wait_send()
        cross_copy(place).wait_send()

        @pl.when(place != z)
        def _():
            line_up(place).wait_send()

        @pl.loop(1, n_sp)
        def _(j):
            x_copy(place, j).wait_send()
            ret_copy(place, j).wait_send()

    @pl.loop(1, tp_size)
    def _(j):
        meta_copy(j).wait_send()


def moe(hidden, meta, shared, norm, experts, cap):
    expert_gate, expert_up, expert_down = experts
    n_sp = lax.axis_size("sp")
    tp_size = lax.axis_size("tp")
    n_z = tp_size // 2
    tokens, width = hidden.shape
    units = expert_gate.shape[2]
    slots = (2 * cap + 15) // 16 * 16
    all_slots = n_sp * slots
    dma = pltpu.SemaphoreType.DMA
    bf16 = jnp.bfloat16
    return pl.pallas_call(
        functools.partial(moe_kernel, n_sp=n_sp, tp_size=tp_size, cap=cap, slots=slots),
        out_shape=jax.ShapeDtypeStruct((tokens, width), bf16),
        in_specs=[pl.BlockSpec(memory_space=pltpu.VMEM)] * 7
        + [pl.BlockSpec(memory_space=pl.ANY)] * 3,
        out_specs=pl.BlockSpec(memory_space=pltpu.VMEM),
        scratch_shapes=[
            pltpu.VMEM((LOCAL_EXPERTS, width, units), bf16),
            pltpu.VMEM((LOCAL_EXPERTS, width, units), bf16),
            pltpu.VMEM((LOCAL_EXPERTS, units, width), bf16),
            pltpu.VMEM((n_z, 2, tokens, width), bf16),
            pltpu.VMEM((tp_size, 4, 128), jnp.float32),
            pltpu.VMEM((n_z, LOCAL_EXPERTS, all_slots, width), bf16),
            pltpu.VMEM((n_z, all_slots, width), bf16),
            pltpu.VMEM((all_slots, units), bf16),
            pltpu.VMEM((n_z, all_slots, width), bf16),
            pltpu.VMEM((n_z, all_slots, width), bf16),
            pltpu.VMEM((tokens, width), jnp.float32),
            pltpu.VMEM((tokens, width), jnp.float32),
            pltpu.VMEM((tp_size, 2, 128), jnp.float32),
            pltpu.VMEM((n_z, tokens, width), bf16),
            pltpu.VMEM((n_z, tokens, width), bf16),
            pltpu.VMEM((n_z + 1, tokens, width), bf16),
            dma((3,)),
            dma((2, n_z)),
            dma((n_z,)),
            dma((n_z,)),
            dma((n_z,)),
            dma((tp_size,)),
            dma((tp_size,)),
            dma((n_z, n_sp)),
            dma((n_z, n_sp)),
            dma((n_z,)),
            dma((n_z,)),
            dma((n_z,)),
            dma((n_z,)),
            dma((n_z, n_sp)),
            dma((n_z, n_sp)),
            dma((n_z,)),
            dma((n_z,)),
            dma((n_z,)),
            dma((n_z + 1,)),
        ],
        compiler_params=pltpu.CompilerParams(
            has_side_effects=True, vmem_limit_bytes=67_000_000
        ),
    )(hidden, meta, *shared, *[vec.reshape(1, width) for vec in norm], expert_gate, expert_up, expert_down)


def local(
    residual,
    wide_query,
    narrow_query,
    wide_keys,
    narrow_keys,
    wide_values,
    narrow_values,
    wide_query_gain,
    wide_key_gain,
    narrow_query_gain,
    narrow_key_gain,
    wide_out,
    narrow_out,
    first_gain,
    first_bias,
    route_ids,
    route_weights,
    expert_gate,
    expert_up,
    expert_down,
    shared_gate,
    shared_up,
    shared_down,
    second_gain,
    second_bias,
):
    hidden = attention(
        (wide_query, narrow_query),
        (wide_keys, narrow_keys, wide_values, narrow_values),
        (wide_query_gain, wide_key_gain, narrow_query_gain, narrow_key_gain),
        residual,
        wide_out,
        narrow_out,
        first_gain,
        first_bias,
    )
    device_rows = hidden.shape[0]
    sp_size = lax.axis_size("sp")
    top_count = route_ids.shape[1]
    experts = LOCAL_EXPERTS * sp_size
    capacity = max(2, (5 * device_rows * top_count + 4 * experts - 1) // (4 * experts))
    meta = jnp.concatenate([route_ids.astype(jnp.float32), route_weights], axis=1)
    meta = jnp.pad(meta, ((0, 128 - device_rows), (0, 0)), constant_values=-1.0).T
    return moe(
        hidden,
        meta,
        (shared_gate, shared_up, shared_down),
        (second_gain, second_bias),
        (expert_gate, expert_up, expert_down),
        capacity,
    )


def solution(mesh):
    in_specs = (
        P(("sp", "tp"), None),
        P("sp", "tp"),
        P("sp", "tp"),
        P("sp", None),
        P("sp", None),
        P("sp", None),
        P("sp", None),
        P(),
        P(),
        P(),
        P(),
        P("tp", None),
        P("tp", None),
        P(),
        P(),
        P(("sp", "tp"), None),
        P(("sp", "tp"), None),
        P("sp", None, "tp"),
        P("sp", None, "tp"),
        P("sp", "tp", None),
        P(),
        P(),
        P(),
        P(),
        P(),
    )
    out_specs = P(("sp", "tp"), None)
    return jax.shard_map(local, mesh=mesh, in_specs=in_specs, out_specs=out_specs, check_vma=False)
```

profile of v0, /device:TPU:11, one launch (start us, length us, event | category | flops | bytes accessed | tf_op | source)
XLA Modules:
  0.0 229.8 jit_solution(889181030058271596)
XLA Ops:
  0.0 0.7 convert_element_type.3
  0.7 1.3 maximum_bitcast_fusion.meta_ref
  2.0 1.5 concatenate.6
  3.4 74.3 %shard_map.307.hidden_ref = bf16[128,2048]{1,0:T(8,128)(2,1)} custom-call(bf16[1024,128]{1,0:T(8,128)(2,1)} %wide_query.1, bf16[1024,128]{1,0:T(8,128)(2,1)} %narrow_query.1, bf16[1024,256]{1,0:T(8,128)(2,1)} %wide_keys.1, bf16[1024,256]{1,0:T(8,128)(2,1)} %narrow_keys.1, bf16[1024,256]{1,0:T(8,128)(2,1)} %wide_values.1, bf16[1024,256]{1,0:T(8,128)(2,1)} %narrow_values.1, ...), custom_call_target="tpu_custom_call" | custom-call | tf_op jit(solution)/shard_map/pallas_call | solution.py:482
  77.7 150.3 %shard_map.308 = bf16[128,2048]{1,0:T(8,128)(2,1)} custom-call(bf16[128,2048]{1,0:T(8,128)(2,1)} %shard_map.307.hidden_ref, f32[4,128]{1,0:T(4,128)} %maximum_bitcast_fusion.meta_ref, bf16[2048,256]{1,0:T(8,128)(2,1)} %shared_gate.1, bf16[2048,256]{1,0:T(8,128)(2,1)} %shared_up.1, bf16[256,2048]{1,0:T(8,128)(2,1)} %shared_down.1, f32[1,2048]{1,0:T(1,128)} %bitcast.10, ...), custom_call_target="tpu_custom_call" | custom-call | tf_op jit(solution)/shard_map/pallas_call | solution.py:1019
  228.0 1.9 copy.35
where the time goes:
time: 230 us
  Pallas kernels  225 us (98%)
  local copies, waits for them, and re-layouts  3.35 us (1%)
    pallas_call x1, Pallas kernels, moe(): pl.pallas_call(functools.partial(moe_kernel, n_sp=n_sp, tp_size=tp_size,...  150 us
    pallas_call x1, Pallas kernels, attention(): pl.pallas_call(functools.partial(attention_kernel, tp_size=tp_size, shard...  74.3 us

commit v1 on v0

--- a/solution.py
+++ b/solution.py
@@ -22,6 +22,25 @@
 EPS_LAYER = 1e-05
 ALPHA = 2.0**0.25
 THETA = 10000.0
+
+
+def greet(tp_size, sp_peers, me_sp, me_tp):
+    barrier = pltpu.get_barrier_semaphore()
+
+    @pl.loop(1, tp_size)
+    def _(j):
+        pl.semaphore_signal(
+            barrier,
+            inc=1,
+            device_id=(me_sp, (me_tp + j) % tp_size),
+            device_id_type=pl.DeviceIdType.MESH,
+        )
+
+    for sp in sp_peers:
+        pl.semaphore_signal(
+            barrier, inc=1, device_id=(sp, me_tp), device_id_type=pl.DeviceIdType.MESH
+        )
+    return lambda: pl.semaphore_wait(barrier, tp_size - 1 + len(sp_peers))
 
 
 def line_order(place, count, step):
@@ -54,7 +73,10 @@
     narrow_keys,
     wide_values,
     narrow_values,
-    gains,
+    wide_query_gain,
+    wide_key_gain,
+    narrow_query_gain,
+    narrow_key_gain,
     wide_row_cos,
     wide_row_sin,
     wide_col_cos,
@@ -144,20 +166,26 @@
         )
 
     def out_piece(place, owner):
-        return out_all.at[2 * place + core, pl.ds(pl.multiple_of(owner * piece, piece), piece)]
-
-    def line_copy(way, d):
-        part = out_piece(z, shard)
-        return remote(
-            part, part, line_send.at[way, d], line_recv.at[z], me_sp, me_tp + (2 - 4 * way) * d
-        )
+        start = (2 * place + core) * 2 * out_rows + owner * piece
+        return out_all.at[pl.ds(pl.multiple_of(start, piece), piece)]
+
+    def line_copy(place, way):
+        part = out_piece(place, shard)
+        return remote(
+            part, part, line_send.at[way, place], line_recv.at[place], me_sp, me_tp + 2 - 4 * way
+        )
+
+    def passes(place, way):
+        if way == 0:
+            return jnp.logical_and(place <= z, z < n_z - 1)
+        return jnp.logical_and(place >= z, z > 0)
 
     def out_pair(place, j):
         part = out_piece(place, (shard - j + shards) % shards)
         return remote(part, part, out_pair_send.at[place, j], out_pair_recv.at[place, j], me_sp, peer)
 
     def own_pair():
-        part = out_all.at[me_tp]
+        part = out_all.at[pl.ds(pl.multiple_of(me_tp * 2 * out_rows, 2 * out_rows), 2 * out_rows)]
         return remote(part, part, out_pair_send.at[z, 0], out_pair_recv.at[z, 0], me_sp, peer)
 
     def share_copy(place, j):
@@ -171,7 +199,7 @@
         target = (me_tp + 1 + b) % tp_size
         return remote(
             mixed.at[kind, target],
-            gathered.at[me_tp, :, pl.ds(kind * lanes, lanes)],
+            gathered.at[:, pl.ds(pl.multiple_of((2 * me_tp + kind) * lanes, lanes), lanes)],
             mixed_send.at[kind, b],
             mixed_recv.at[kind, b],
             me_sp,
@@ -180,14 +208,35 @@
 
     loads = [
         pltpu.make_async_copy(
-            src, out_all.at[me_tp, pl.ds(i * out_rows, out_rows)], load_sem.at[i]
+            src,
+            out_all.at[pl.ds(pl.multiple_of((2 * me_tp + i) * out_rows, out_rows), out_rows)],
+            load_sem.at[i],
         )
         for i, src in enumerate((wide_out, narrow_out))
     ]
+    await_peers = greet(
+        tp_size, [first_sp + (shard + j) % shards for j in range(1, shards)], me_sp, me_tp
+    )
     for copy in loads:
         copy.start()
 
     lane = lax.broadcasted_iota(jnp.int32, (1, lanes), 1)
+
+    def spread_gain(gain):
+        size = gain.shape[1]
+        row = lax.broadcasted_iota(jnp.int32, (size, lanes), 0)
+        column = lax.broadcasted_iota(jnp.int32, (size, lanes), 1)
+        return jnp.dot(
+            jnp.broadcast_to(gain[...], (8, size)),
+            jnp.where(column % size == row, 1.0, 0.0),
+            precision=lax.Precision.HIGHEST,
+            preferred_element_type=jnp.float32,
+        )[0:1]
+
+    gains = [
+        spread_gain(gain)
+        for gain in (wide_query_gain, wide_key_gain, narrow_query_gain, narrow_key_gain)
+    ]
 
     def normalized(values, size, gain_row, row_cos, row_sin, col_cos, col_sin, i):
         squares = values * values
@@ -199,7 +248,7 @@
         total = jnp.dot(high, same, preferred_element_type=jnp.float32) + jnp.dot(
             low, same, preferred_element_type=jnp.float32
         )
-        scaled = values * lax.rsqrt(total * (1.0 / size) + EPS_HEAD) * gains[gain_row : gain_row + 1, :]
+        scaled = values * lax.rsqrt(total * (1.0 / size) + EPS_HEAD) * gains[gain_row]
         quarter = size // 4
         partner = jnp.where(
             lane % (size // 2) < quarter,
@@ -244,6 +293,7 @@
     def _(i):
         key_step(0, i, wide_keys, wide_values, wide_picks, wide_size, 1, wide_tables)
 
+    await_peers()
     for j in range(1, shards):
         kv_copy(0, j).start()
 
@@ -251,15 +301,11 @@
         copy.wait()
     own_pair().start()
 
-    for d in range(1, n_z):
-
-        @pl.when(z + d < n_z)
-        def _():
-            line_copy(0, d).start()
-
-        @pl.when(z - d >= 0)
-        def _():
-            line_copy(1, d).start()
+    for way in range(2):
+
+        @pl.when(passes(z, way))
+        def _():
+            line_copy(z, way).start()
 
     @pl.loop(0, blocks)
     def _(i):
@@ -318,24 +364,46 @@
 
         @pl.when(b == tp_size - 1)
         def _():
-            gathered[target, :, kind * lanes : (kind + 1) * lanes] = value
+            spot = pl.multiple_of((2 * target + kind) * lanes, lanes)
+            gathered[:, pl.ds(spot, lanes)] = value
+
+    def line_wait(place):
+        part = out_piece(place, shard)
+        pltpu.make_async_copy(part, part, line_recv.at[place]).wait()
+
+    def forward_step(step):
+        place = line_order(z, n_z, step)
+        for way in range(2):
+
+            @pl.when(passes(place, way))
+            def _():
+                line_wait(place)
+                line_copy(place, way).start()
 
     def share_step(step):
         place = line_order(z, n_z, step)
-        part = out_piece(place, shard)
-        pltpu.make_async_copy(part, part, line_recv.at[place]).wait()
+
+        @pl.when(jnp.logical_not(jnp.logical_or(passes(place, 0), passes(place, 1))))
+        def _():
+            line_wait(place)
+
         for j in range(1, shards):
             share_copy(place, j).start()
         out_pair(place, 0).start()
 
-    early = (tp_size - tp_size // 2 + 2) // 3
     relay_kv(0)
+    for step in range(1, min(3, n_z)):
+        forward_step(step)
 
     @pl.loop(0, tp_size)
     def _(b):
-        @pl.when(jnp.logical_and(b >= tp_size // 2, (b - tp_size // 2) % 3 == 0))
-        def _():
-            share_step((b - tp_size // 2) // 3 + 1)
+        @pl.when(jnp.logical_and(b >= n_z, b < 2 * n_z - 3))
+        def _():
+            forward_step(b - n_z + 3)
+
+        @pl.when(jnp.logical_or(b == n_z // 2, b == n_z + n_z // 2))
+        def _():
+            share_step(b // n_z + 1)
 
         target = (me_tp + 1 + b) % tp_size
         rows = pl.ds(pl.multiple_of(target * tokens, tokens), tokens)
@@ -353,9 +421,9 @@
 
     @pl.loop(0, tp_size)
     def _(b):
-        @pl.when(jnp.logical_and(b > 0, b + early < n_z))
-        def _():
-            share_step(b + early)
+        @pl.when(jnp.logical_and(b > 0, b + 2 < n_z))
+        def _():
+            share_step(b + 2)
 
         @pl.when(b > tp_size - n_z)
         def _():
@@ -398,24 +466,19 @@
     chunk = 512
     for start in range(0, width, chunk):
 
-        def add(q, total):
-            if out_rows == lanes:
-                return total + jnp.dot(
-                    gathered[q],
-                    out_all[q, :, start : start + chunk],
+        total = ALPHA * residual[:, start : start + chunk].astype(jnp.float32)
+        if out_rows == lanes:
+            total = total + jnp.dot(
+                gathered[...], out_all[:, start : start + chunk], preferred_element_type=jnp.float32
+            )
+        else:
+            for q in range(2 * tp_size):
+                total = total + jnp.dot(
+                    gathered[:, q * lanes : q * lanes + out_rows],
+                    out_all[q * out_rows : (q + 1) * out_rows, start : start + chunk],
                     preferred_element_type=jnp.float32,
                 )
-            for kind in range(2):
-                total = total + jnp.dot(
-                    gathered[q, :, kind * lanes : kind * lanes + out_rows],
-                    out_all[q, kind * out_rows : (kind + 1) * out_rows, start : start + chunk],
-                    preferred_element_type=jnp.float32,
-                )
-            return total
-
-        projected[:, start : start + chunk] = lax.fori_loop(
-            0, tp_size, add, ALPHA * residual[:, start : start + chunk].astype(jnp.float32)
-        )
+        projected[:, start : start + chunk] = total
 
     values = projected[...]
     center = jnp.mean(values, axis=-1, keepdims=True)
@@ -433,13 +496,11 @@
 
     @pl.loop(0, n_z)
     def _(place):
-        @pl.when(jnp.logical_and(place > 0, z + place < n_z))
-        def _():
-            line_copy(0, place).wait_send()
-
-        @pl.when(jnp.logical_and(place > 0, z - place >= 0))
-        def _():
-            line_copy(1, place).wait_send()
+        for way in range(2):
+
+            @pl.when(passes(place, way))
+            def _():
+                line_copy(place, way).wait_send()
 
         @pl.when(place != z)
         def _():
@@ -466,9 +527,7 @@
     sizes = gain_vecs[0].shape[0], gain_vecs[2].shape[0]
     local_heads = [q.shape[1] // size for q, size in zip(queries, sizes)]
     queries = [jnp.pad(q, ((0, 0), (0, lanes - q.shape[1]))) for q in queries]
-    gains = jnp.concatenate(
-        [gain for gain in gain_vecs for _ in range(lanes // gain.shape[0])]
-    ).reshape(len(gain_vecs), lanes)
+    gains = [gain.reshape(1, -1) for gain in gain_vecs]
     grid_rows = shards * seg_rows // GRID_WIDTH
     tables = [
         jnp.asarray(table)
@@ -490,7 +549,7 @@
             local_narrow=local_heads[1],
         ),
         out_shape=jax.ShapeDtypeStruct((tokens, width), bf16),
-        in_specs=[vmem] * 16 + [hbm] * 2 + [vmem] * 2,
+        in_specs=[vmem] * 19 + [hbm] * 2 + [vmem] * 2,
         out_specs=vmem,
         scratch_shapes=[
             pltpu.VMEM((shards * seg_rows, lanes), bf16),
@@ -498,9 +557,9 @@
             pltpu.VMEM((shards * seg_rows, lanes), bf16),
             pltpu.VMEM((local_heads[0], seg_rows, lanes), bf16),
             pltpu.VMEM((local_heads[1], seg_rows, lanes), bf16),
-            pltpu.VMEM((tp_size, 2 * wide_out.shape[0], width), bf16),
+            pltpu.VMEM((2 * tp_size * wide_out.shape[0], width), bf16),
             pltpu.VMEM((2, tp_size, tokens, lanes), bf16),
-            pltpu.VMEM((tp_size, tokens, 2 * lanes), bf16),
+            pltpu.VMEM((tokens, 2 * tp_size * lanes), bf16),
             pltpu.VMEM((tokens, width), jnp.float32),
             dma((2,)),
             dma((2, shards)),
@@ -517,12 +576,12 @@
             dma((2, tp_size)),
         ],
         compiler_params=pltpu.CompilerParams(
-            has_side_effects=True, vmem_limit_bytes=66_000_000
+            collective_id=0, has_side_effects=True, vmem_limit_bytes=66_000_000
         ),
     )(
         *queries,
         *keys_values,
-        gains,
+        *gains,
         *tables,
         residual,
         wide_out,
@@ -535,11 +594,11 @@
 def moe_kernel(
     hidden_ref,
     meta_ref,
-    shared_gate,
-    shared_up,
-    shared_down,
     norm_gain,
     norm_bias,
+    shared_gate_hbm,
+    shared_up_hbm,
+    shared_down_hbm,
     gate_hbm,
     up_hbm,
     down_hbm,
@@ -547,6 +606,9 @@
     gate_ref,
     up_ref,
     down_ref,
+    shared_gate,
+    shared_up,
+    shared_down,
     hid,
     meta_all,
     rows,
@@ -560,6 +622,9 @@
     cross_send,
     cross,
     line_in,
+    far_in,
+    far_line_in,
+    far_sum,
     weight_sem,
     z_send,
     z_recv,
@@ -579,22 +644,41 @@
     cross_recv,
     line_send,
     line_recv,
+    far_send_sem,
+    far_line_send,
+    far_line_recv,
     *,
     n_sp,
     tp_size,
     cap,
     slots,
+    by_line,
 ):
     n_z = tp_size // 2
     tokens, width = hidden_ref.shape
     all_slots = n_sp * slots
     chunk = 512
+    lag = 2
     expert_lines = (LOCAL_EXPERTS * n_sp + 15) // 16 * 16
     me_sp = lax.axis_index("sp")
     me_tp = lax.axis_index("tp")
     z = me_tp // 2
     core = me_tp % 2
     peer = me_tp + 1 - 2 * core
+    far_sp = n_sp - 1 - me_sp
+    far_send = (2 * n_sp - 1 - 2 * me_sp) % n_sp
+    far_recv = (2 * me_sp + 1) % n_sp
+    relays = core == 1 if by_line else False
+
+    def skipped(j, far_j, place):
+        if not by_line:
+            return j < 0
+        return jnp.logical_and(core == 1, jnp.logical_and(j == far_j, place != z))
+
+    def is_far(j, far_j):
+        if not by_line:
+            return j < 0
+        return jnp.logical_and(core == 1, j == far_j)
 
     def remote(src, dst, send_sem, recv_sem, sp, tp):
         return pltpu.make_async_remote_copy(
@@ -609,7 +693,14 @@
     weight_copies = [
         pltpu.make_async_copy(src, dst, weight_sem.at[i])
         for i, (src, dst) in enumerate(
-            ((gate_hbm, gate_ref), (up_hbm, up_ref), (down_hbm, down_ref))
+            (
+                (shared_gate_hbm, shared_gate),
+                (shared_up_hbm, shared_up),
+                (shared_down_hbm, shared_down),
+                (gate_hbm, gate_ref),
+                (up_hbm, up_ref),
+                (down_hbm, down_ref),
+            )
         )
     ]
 
@@ -652,6 +743,42 @@
             me_tp,
         )
 
+    def far_copy(place):
+        return remote(
+            stage.at[place, slot_rows(far_sp)],
+            far_in.at[place],
+            x_send.at[place, far_send],
+            x_recv.at[place, far_send],
+            far_sp,
+            me_tp,
+        )
+
+    def far_relay(place, way):
+        return remote(
+            far_in.at[place],
+            far_in.at[place],
+            far_send_sem.at[way, place],
+            x_recv.at[place, far_recv],
+            me_sp,
+            me_tp + 2 - 4 * way,
+        )
+
+    def far_line(place, way):
+        spot = place if way == 0 else jnp.where(place == z - 1, n_z, place)
+        return remote(
+            rows.at[place, core, slot_rows(far_sp)],
+            far_line_in.at[spot],
+            far_line_send.at[place],
+            far_line_recv.at[spot],
+            me_sp,
+            me_tp + 2 - 4 * way,
+        )
+
+    def passes(place, way):
+        if way == 0:
+            return jnp.logical_and(place <= z, z < n_z - 1)
+        return jnp.logical_and(place >= z, z > 0)
+
     def rows_copy(place):
         return remote(
             rows.at[place, core],
@@ -704,24 +831,27 @@
             cross.at[place], line_in.at[spot], line_send.at[place], line_recv.at[spot], me_sp, me_tp - 2
         )
 
-    pair_copy(hidden_ref, z).start()
-
-    @pl.when(z < n_z - 1)
-    def _():
-        line_copy(hidden_ref, 0, z).start()
-
-    @pl.when(z > 0)
-    def _():
-        line_copy(hidden_ref, 1, z).start()
-
-    @pl.loop(1, tp_size)
-    def _(j):
-        meta_copy(j).start()
-
+    await_peers = greet(
+        tp_size, [(me_sp + j) % n_sp for j in range(1, n_sp)], me_sp, me_tp
+    )
     for copy in weight_copies:
         copy.start()
     hid[z, core] = hidden_ref[...]
     meta_all[me_tp] = meta_ref[...]
+    await_peers()
+    pair_copy(hidden_ref, z).start()
+
+    @pl.when(z < n_z - 1)
+    def _():
+        line_copy(hidden_ref, 0, z).start()
+
+    @pl.when(z > 0)
+    def _():
+        line_copy(hidden_ref, 1, z).start()
+
+    @pl.loop(1, tp_size)
+    def _(j):
+        meta_copy(j).start()
 
     def selection(place, sp, weighted):
         expert = (LOCAL_EXPERTS * sp + core).astype(jnp.float32)
@@ -739,7 +869,20 @@
             parts.append(part)
         return jnp.concatenate(parts, axis=1)
 
+    def clear_far():
+        if by_line:
+
+            @pl.when(core == 1)
+            def _():
+                @pl.loop(0, n_z)
+                def _(place):
+                    @pl.when(place != z)
+                    def _():
+                        ret[place, slot_rows(far_sp)] = jnp.zeros((slots, width), jnp.bfloat16)
+
     def shared_expert():
+        for copy in weight_copies[:3]:
+            copy.wait()
         gate_values = jnp.dot(hidden_ref[...], shared_gate[...], preferred_element_type=jnp.float32)
         up_values = jnp.dot(hidden_ref[...], shared_up[...], preferred_element_type=jnp.float32)
         active = (jax.nn.silu(gate_values) * up_values).astype(jnp.bfloat16)
@@ -793,25 +936,34 @@
         def _(i):
             j = (i + 1) % n_sp
             sp = (me_sp + j) % n_sp
-            picks = selection(place, sp, False).astype(jnp.bfloat16)
-            for start in range(0, width, chunk):
-                piece = (
-                    jnp.dot(
-                        picks[:, :tokens],
-                        hid[place, 0, :, start : start + chunk],
-                        preferred_element_type=jnp.float32,
-                    )
-                    + jnp.dot(
-                        picks[:, tokens:],
-                        hid[place, 1, :, start : start + chunk],
-                        preferred_element_type=jnp.float32,
-                    )
-                ).astype(jnp.bfloat16)
-                stage[place, slot_rows(sp), start : start + chunk] = piece
-
-            @pl.when(j > 0)
-            def _():
-                x_copy(place, j).start()
+
+            @pl.when(jnp.logical_not(skipped(j, far_send, place)))
+            def _():
+                picks = selection(place, sp, False).astype(jnp.bfloat16)
+                for start in range(0, width, chunk):
+                    piece = (
+                        jnp.dot(
+                            picks[:, :tokens],
+                            hid[place, 0, :, start : start + chunk],
+                            preferred_element_type=jnp.float32,
+                        )
+                        + jnp.dot(
+                            picks[:, tokens:],
+                            hid[place, 1, :, start : start + chunk],
+                            preferred_element_type=jnp.float32,
+                        )
+                    ).astype(jnp.bfloat16)
+                    stage[place, slot_rows(sp), start : start + chunk] = piece
+
+                @pl.when(jnp.logical_and(j > 0, jnp.logical_not(is_far(j, far_send))))
+                def _():
+                    x_copy(place, j).start()
+
+                if by_line:
+
+                    @pl.when(is_far(j, far_send))
+                    def _():
+                        far_copy(place).start()
 
             @pl.when(j == 0)
             def _():
@@ -820,9 +972,35 @@
     def compute_step(step):
         place = line_order(z, n_z, step)
 
+        if by_line:
+
+            def start_relay(place):
+                for way in range(2):
+
+                    @pl.when(passes(place, way))
+                    def _():
+                        far_relay(place, way).start()
+
+            @pl.when(relays)
+            def _():
+                @pl.when(step == n_z - 1 - lag)
+                def _():
+                    for earlier in range(n_z - 1 - lag):
+                        start_relay(line_order(z, n_z, earlier))
+
+                far_relay(place, 0).wait_recv()
+
+                @pl.when(step >= n_z - 1 - lag)
+                def _():
+                    start_relay(place)
+
+                rows[place, core, slot_rows(far_sp)] = far_in[place]
+
         @pl.loop(1, n_sp)
         def _(j):
-            x_copy(place, j).wait_recv()
+            @pl.when(jnp.logical_not(is_far(j, far_recv)))
+            def _():
+                x_copy(place, j).wait_recv()
 
         rows_copy(place).start()
 
@@ -839,14 +1017,13 @@
                 ).astype(jnp.bfloat16)
 
         expert(core)
-        rows_copy(place).wait()
+        rows_copy(place).wait_send()
         finish(core)
+        rows_copy(place).wait_recv()
         expert(1 - core)
         finish(1 - core)
         part_copy(place).start()
 
-    lag = 2
-
     @pl.loop(0, n_z + lag)
     def _(step):
         @pl.when(step < n_z)
@@ -855,11 +1032,13 @@
 
         @pl.when(step == 0)
         def _():
+            if by_line:
+                clear_far()
             shared_expert()
 
         @pl.when(step == lag)
         def _():
-            for copy in weight_copies:
+            for copy in weight_copies[3:]:
                 copy.wait()
 
         @pl.when(step >= lag)
@@ -874,26 +1053,68 @@
         def _(i):
             j = (i + 1) % n_sp
             sp = (me_sp + j) % n_sp
-            total = (
-                rows[place, core, slot_rows(sp)].astype(jnp.float32)
-                + peer_part[place, slot_rows(sp)].astype(jnp.float32)
-            ).astype(jnp.bfloat16)
-
-            @pl.when(j > 0)
-            def _():
-                rows[place, core, slot_rows(sp)] = total
-                ret_copy(place, j).start()
-
-            @pl.when(j == 0)
-            def _():
-                ret[place, slot_rows(me_sp)] = total
+
+            @pl.when(jnp.logical_not(is_far(j, far_send)))
+            def _():
+                total = (
+                    rows[place, core, slot_rows(sp)].astype(jnp.float32)
+                    + peer_part[place, slot_rows(sp)].astype(jnp.float32)
+                ).astype(jnp.bfloat16)
+
+                @pl.when(j > 0)
+                def _():
+                    rows[place, core, slot_rows(sp)] = total
+                    ret_copy(place, j).start()
+
+                @pl.when(j == 0)
+                def _():
+                    ret[place, slot_rows(me_sp)] = total
+
+        if by_line:
+
+            @pl.when(relays)
+            def _():
+                far_sum[...] = rows[place, core, slot_rows(far_sp)].astype(jnp.float32) + peer_part[
+                    place, slot_rows(far_sp)
+                ].astype(jnp.float32)
+
+                @pl.when(jnp.logical_and(z > 0, place >= z))
+                def _():
+                    pltpu.make_async_copy(
+                        far_in.at[place], far_line_in.at[place], far_line_recv.at[place]
+                    ).wait()
+                    far_sum[...] = far_sum[...] + far_line_in[place].astype(jnp.float32)
+
+                @pl.when(jnp.logical_and(z < n_z - 1, place <= z))
+                def _():
+                    spot = jnp.where(place == z, n_z, place)
+                    pltpu.make_async_copy(
+                        far_in.at[place], far_line_in.at[spot], far_line_recv.at[spot]
+                    ).wait()
+                    far_sum[...] = far_sum[...] + far_line_in[spot].astype(jnp.float32)
+
+                rows[place, core, slot_rows(far_sp)] = far_sum[...].astype(jnp.bfloat16)
+
+                @pl.when(place == z)
+                def _():
+                    ret_copy(place, far_send).start()
+
+                @pl.when(place > z)
+                def _():
+                    far_line(place, 0).start()
+
+                @pl.when(place < z)
+                def _():
+                    far_line(place, 1).start()
 
     def combine_step(step):
         place = line_order(z, n_z, n_z - 1 - step)
 
         @pl.loop(1, n_sp)
         def _(j):
-            ret_copy(place, j).wait_recv()
+            @pl.when(jnp.logical_not(skipped(j, far_recv, place)))
+            def _():
+                ret_copy(place, j).wait_recv()
 
         for lane in range(2):
             info = meta_all[2 * place + lane]
@@ -997,8 +1218,24 @@
 
         @pl.loop(1, n_sp)
         def _(j):
-            x_copy(place, j).wait_send()
-            ret_copy(place, j).wait_send()
+            @pl.when(jnp.logical_not(skipped(j, far_send, place)))
+            def _():
+                x_copy(place, j).wait_send()
+                ret_copy(place, j).wait_send()
+
+        if by_line:
+
+            @pl.when(relays)
+            def _():
+                for way in range(2):
+
+                    @pl.when(passes(place, way))
+                    def _():
+                        far_relay(place, way).wait_send()
+
+                @pl.when(place != z)
+                def _():
+                    far_line(place, 0).wait_send()
 
     @pl.loop(1, tp_size)
     def _(j):
@@ -1014,18 +1251,22 @@
     units = expert_gate.shape[2]
     slots = (2 * cap + 15) // 16 * 16
     all_slots = n_sp * slots
+    by_line = n_sp == 4
     dma = pltpu.SemaphoreType.DMA
     bf16 = jnp.bfloat16
     return pl.pallas_call(
-        functools.partial(moe_kernel, n_sp=n_sp, tp_size=tp_size, cap=cap, slots=slots),
+        functools.partial(
+            moe_kernel, n_sp=n_sp, tp_size=tp_size, cap=cap, slots=slots, by_line=by_line
+        ),
         out_shape=jax.ShapeDtypeStruct((tokens, width), bf16),
-        in_specs=[pl.BlockSpec(memory_space=pltpu.VMEM)] * 7
-        + [pl.BlockSpec(memory_space=pl.ANY)] * 3,
+        in_specs=[pl.BlockSpec(memory_space=pltpu.VMEM)] * 4
+        + [pl.BlockSpec(memory_space=pl.ANY)] * 6,
         out_specs=pl.BlockSpec(memory_space=pltpu.VMEM),
         scratch_shapes=[
             pltpu.VMEM((LOCAL_EXPERTS, width, units), bf16),
             pltpu.VMEM((LOCAL_EXPERTS, width, units), bf16),
             pltpu.VMEM((LOCAL_EXPERTS, units, width), bf16),
+            *[pltpu.VMEM(weight.shape, bf16) for weight in shared],
             pltpu.VMEM((n_z, 2, tokens, width), bf16),
             pltpu.VMEM((tp_size, 4, 128), jnp.float32),
             pltpu.VMEM((n_z, LOCAL_EXPERTS, all_slots, width), bf16),
@@ -1039,7 +1280,10 @@
             pltpu.VMEM((n_z, tokens, width), bf16),
             pltpu.VMEM((n_z, tokens, width), bf16),
             pltpu.VMEM((n_z + 1, tokens, width), bf16),
-            dma((3,)),
+            pltpu.VMEM((n_z, slots, width) if by_line else (1, 16, 128), bf16),
+            pltpu.VMEM((n_z + 1, slots, width) if by_line else (1, 16, 128), bf16),
+            pltpu.VMEM((slots, width) if by_line else (8, 128), jnp.float32),
+            dma((6,)),
             dma((2, n_z)),
             dma((n_z,)),
             dma((n_z,)),
@@ -1058,11 +1302,14 @@
             dma((n_z,)),
             dma((n_z,)),
             dma((n_z + 1,)),
+            dma((2, n_z)),
+            dma((n_z,)),
+            dma((n_z + 1,)),
         ],
         compiler_params=pltpu.CompilerParams(
-            has_side_effects=True, vmem_limit_bytes=67_000_000
+            collective_id=1, has_side_effects=True, vmem_limit_bytes=67_000_000
         ),
-    )(hidden, meta, *shared, *[vec.reshape(1, width) for vec in norm], expert_gate, expert_up, expert_down)
+    )(hidden, meta, *[vec.reshape(1, width) for vec in norm], *shared, expert_gate, expert_up, expert_down)
 
 
 def local(

time: 230 us -> 207 us (0.900)
  Pallas kernels: 225 us -> 202 us
    pallas_call x1, Pallas kernels: 74.3 us -> 60.5 us  [attention(): pl.pallas_call(functools.partial(attention_kernel, tp_size=tp_size, shard...]
    pallas_call x1, Pallas kernels: 150 us -> 141 us  [moe(): pl.pallas_call(functools.partial(moe_kernel, n_sp=n_sp, tp_size=tp_size,...]
where the time goes in v1:
time: 207 us; the launch traced here: 206 us
  Pallas kernels  202 us (98%)
    pallas_call x1, Pallas kernels, moe(): pl.pallas_call(functools.partial(moe_kernel, n_sp=n_sp, tp_size=tp_size,...  141 us
    pallas_call x1, Pallas kernels, attention(): pl.pallas_call(functools.partial(attention_kernel, tp_size=tp_size, shard...  60.5 us

profile of v1, /device:TPU:11, one launch (start us, length us, event | category | flops | bytes accessed | tf_op | source)
XLA Modules:
  0.0 205.8 jit_solution(3796163752479504425)
XLA Ops:
  0.0 0.7 convert_element_type.3
  0.7 1.3 maximum_bitcast_fusion.meta_ref
  1.9 60.5 %shard_map.307.hidden_ref = bf16[128,2048]{1,0:T(8,128)(2,1)} custom-call(bf16[1024,128]{1,0:T(8,128)(2,1)} %wide_query.1, bf16[1024,128]{1,0:T(8,128)(2,1)} %narrow_query.1, bf16[1024,256]{1,0:T(8,128)(2,1)} %wide_keys.1, bf16[1024,256]{1,0:T(8,128)(2,1)} %narrow_keys.1, bf16[1024,256]{1,0:T(8,128)(2,1)} %wide_values.1, bf16[1024,256]{1,0:T(8,128)(2,1)} %narrow_values.1, ...), custom_call_target="tpu_custom_call" | custom-call | tf_op jit(solution)/shard_map/pallas_call | solution.py:541
  62.5 141.4 %shard_map.308 = bf16[128,2048]{1,0:T(8,128)(2,1)} custom-call(bf16[128,2048]{1,0:T(8,128)(2,1)} %shard_map.307.hidden_ref, f32[4,128]{1,0:T(4,128)} %maximum_bitcast_fusion.meta_ref, f32[1,2048]{1,0:T(1,128)} %bitcast.12, f32[1,2048]{1,0:T(1,128)} %bitcast.13, bf16[2048,256]{1,0:T(8,128)(2,1)} %shared_gate_hbm.1, bf16[2048,256]{1,0:T(8,128)(2,1)} %shared_up_hbm.1, ...), custom_call_target="tpu_custom_call" | custom-call | tf_op jit(solution)/shard_map/pallas_call | solution.py:1257
  203.9 1.9 copy.35

commit v2 on v1

--- a/solution.py
+++ b/solution.py
@@ -341,10 +341,12 @@
         sums = jnp.dot(weights, values_ones[...], preferred_element_type=jnp.float32)
         return sums / sums[:, 0:1]
 
-    def relay_kv(kind):
+    def forward_kv(kind):
         for j in range(1, shards):
             kv_copy(kind, j).wait_recv()
             kv_pair(kind, j).start()
+
+    def arrived_kv(kind):
         for j in range(1, shards):
             kv_pair(kind, j).wait_recv()
         size = (wide_size, narrow_size)[kind]
@@ -391,12 +393,17 @@
             share_copy(place, j).start()
         out_pair(place, 0).start()
 
-    relay_kv(0)
+    forward_kv(0)
+    arrived_kv(0)
     for step in range(1, min(3, n_z)):
         forward_step(step)
 
     @pl.loop(0, tp_size)
     def _(b):
+        @pl.when(b == n_z - 1)
+        def _():
+            forward_kv(1)
+
         @pl.when(jnp.logical_and(b >= n_z, b < 2 * n_z - 3))
         def _():
             forward_step(b - n_z + 3)
@@ -417,7 +424,7 @@
             total = total + jnp.where(lane // wide_size == h, moved, 0.0)
         put_mixed(0, b, target, total.astype(jnp.bfloat16))
 
-    relay_kv(1)
+    arrived_kv(1)
 
     @pl.loop(0, tp_size)
     def _(b):
@@ -659,6 +666,8 @@
     all_slots = n_sp * slots
     chunk = 512
     lag = 2
+    parts = 4
+    cuts = 2
     expert_lines = (LOCAL_EXPERTS * n_sp + 15) // 16 * 16
     me_sp = lax.axis_index("sp")
     me_tp = lax.axis_index("tp")
@@ -704,12 +713,13 @@
         )
     ]
 
-    def line_copy(src, way, place):
-        return remote(
-            src,
-            hid.at[place, core],
-            z_send.at[way, place],
-            z_recv.at[place],
+    def line_copy(src, way, place, h):
+        lines = pl.ds(h * (tokens // cuts), tokens // cuts)
+        return remote(
+            src.at[lines],
+            hid.at[place, core, lines],
+            z_send.at[cuts * way + h, place],
+            z_recv.at[h, place],
             me_sp,
             me_tp + 2 - 4 * way,
         )
@@ -810,25 +820,30 @@
             me_tp,
         )
 
-    def cross_copy(place):
-        return remote(
-            cross_send.at[place],
-            cross.at[place],
-            cross_send_sem.at[place],
-            cross_recv.at[place],
+    half_width = width // parts
+
+    def columns(h):
+        return pl.ds(h * half_width, half_width)
+
+    def cross_copy(place, h):
+        return remote(
+            cross_send.at[place, :, columns(h)],
+            cross.at[place, :, columns(h)],
+            cross_send_sem.at[h, place],
+            cross_recv.at[h, place],
             me_sp,
             peer,
         )
 
-    def line_up(place):
-        return remote(
-            cross.at[place], line_in.at[place], line_send.at[place], line_recv.at[place], me_sp, me_tp + 2
-        )
-
-    def line_dn(place):
-        spot = jnp.where(place == z - 1, n_z, place)
-        return remote(
-            cross.at[place], line_in.at[spot], line_send.at[place], line_recv.at[spot], me_sp, me_tp - 2
+    def sum_copy(place, way, h):
+        spot = place if way == 0 else jnp.where(place == z - 1, n_z, place)
+        return remote(
+            cross.at[place, :, columns(h)],
+            line_in.at[spot, :, columns(h)],
+            line_send.at[h, place],
+            line_recv.at[h, spot],
+            me_sp,
+            me_tp + 2 - 4 * way,
         )
 
     await_peers = greet(
@@ -841,13 +856,15 @@
     await_peers()
     pair_copy(hidden_ref, z).start()
 
-    @pl.when(z < n_z - 1)
-    def _():
-        line_copy(hidden_ref, 0, z).start()
-
-    @pl.when(z > 0)
-    def _():
-        line_copy(hidden_ref, 1, z).start()
+    for h in range(cuts):
+
+        @pl.when(z < n_z - 1)
+        def _():
+            line_copy(hidden_ref, 0, z, h).start()
+
+        @pl.when(z > 0)
+        def _():
+            line_copy(hidden_ref, 1, z, h).start()
 
     @pl.loop(1, tp_size)
     def _(j):
@@ -897,15 +914,19 @@
 
         @pl.when(step > 0)
         def _():
-            pltpu.make_async_copy(hidden_ref, hid.at[place, core], z_recv.at[place]).wait()
-
-            @pl.when(jnp.logical_and(place < z, z < n_z - 1))
-            def _():
-                line_copy(hid.at[place, core], 0, place).start()
-
-            @pl.when(jnp.logical_and(place > z, z > 0))
-            def _():
-                line_copy(hid.at[place, core], 1, place).start()
+            for h in range(cuts):
+                lines = pl.ds(h * (tokens // cuts), tokens // cuts)
+                pltpu.make_async_copy(
+                    hidden_ref.at[lines], hid.at[place, core, lines], z_recv.at[h, place]
+                ).wait()
+
+                @pl.when(jnp.logical_and(place < z, z < n_z - 1))
+                def _():
+                    line_copy(hid.at[place, core], 0, place, h).start()
+
+                @pl.when(jnp.logical_and(place > z, z > 0))
+                def _():
+                    line_copy(hid.at[place, core], 1, place, h).start()
 
             pair_copy(hid.at[place, core], place).start()
 
@@ -1070,42 +1091,41 @@
                 def _():
                     ret[place, slot_rows(me_sp)] = total
 
-        if by_line:
-
-            @pl.when(relays)
-            def _():
-                far_sum[...] = rows[place, core, slot_rows(far_sp)].astype(jnp.float32) + peer_part[
-                    place, slot_rows(far_sp)
-                ].astype(jnp.float32)
-
-                @pl.when(jnp.logical_and(z > 0, place >= z))
-                def _():
-                    pltpu.make_async_copy(
-                        far_in.at[place], far_line_in.at[place], far_line_recv.at[place]
-                    ).wait()
-                    far_sum[...] = far_sum[...] + far_line_in[place].astype(jnp.float32)
-
-                @pl.when(jnp.logical_and(z < n_z - 1, place <= z))
-                def _():
-                    spot = jnp.where(place == z, n_z, place)
-                    pltpu.make_async_copy(
-                        far_in.at[place], far_line_in.at[spot], far_line_recv.at[spot]
-                    ).wait()
-                    far_sum[...] = far_sum[...] + far_line_in[spot].astype(jnp.float32)
-
-                rows[place, core, slot_rows(far_sp)] = far_sum[...].astype(jnp.bfloat16)
-
-                @pl.when(place == z)
-                def _():
-                    ret_copy(place, far_send).start()
-
-                @pl.when(place > z)
-                def _():
-                    far_line(place, 0).start()
-
-                @pl.when(place < z)
-                def _():
-                    far_line(place, 1).start()
+    def far_step(step):
+        place = line_order(z, n_z, n_z - 1 - step)
+
+        far_sum[...] = rows[place, core, slot_rows(far_sp)].astype(jnp.float32) + peer_part[
+            place, slot_rows(far_sp)
+        ].astype(jnp.float32)
+
+        @pl.when(jnp.logical_and(z > 0, place >= z))
+        def _():
+            pltpu.make_async_copy(
+                far_in.at[place], far_line_in.at[place], far_line_recv.at[place]
+            ).wait()
+            far_sum[...] = far_sum[...] + far_line_in[place].astype(jnp.float32)
+
+        @pl.when(jnp.logical_and(z < n_z - 1, place <= z))
+        def _():
+            spot = jnp.where(place == z, n_z, place)
+            pltpu.make_async_copy(
+                far_in.at[place], far_line_in.at[spot], far_line_recv.at[spot]
+            ).wait()
+            far_sum[...] = far_sum[...] + far_line_in[spot].astype(jnp.float32)
+
+        rows[place, core, slot_rows(far_sp)] = far_sum[...].astype(jnp.bfloat16)
+
+        @pl.when(place == z)
+        def _():
+            ret_copy(place, far_send).start()
+
+        @pl.when(place > z)
+        def _():
+            far_line(place, 0).start()
+
+        @pl.when(place < z)
+        def _():
+            far_line(place, 1).start()
 
     def combine_step(step):
         place = line_order(z, n_z, n_z - 1 - step)
@@ -1116,6 +1136,7 @@
             def _():
                 ret_copy(place, j).wait_recv()
 
+        splits = []
         for lane in range(2):
             info = meta_all[2 * place + lane]
             lines = lax.broadcasted_iota(jnp.int32, (all_slots, tokens), 0).astype(jnp.float32)
@@ -1131,41 +1152,59 @@
                     lines == target, info[2 + choice : 3 + choice, :tokens], 0.0
                 )
             high = picks.astype(jnp.bfloat16)
-            low = (picks - high.astype(jnp.float32)).astype(jnp.bfloat16)
-
-            for start in range(0, width, chunk):
-                piece = sum(
-                    lax.dot_general(
-                        part,
-                        ret[place, :, start : start + chunk],
-                        (((0,), (0,)), ((), ())),
-                        preferred_element_type=jnp.float32,
+            splits.append((high, (picks - high.astype(jnp.float32)).astype(jnp.bfloat16)))
+
+        for h in range(parts):
+            for lane in range(2):
+                for start in range(h * half_width, (h + 1) * half_width, chunk):
+                    piece = sum(
+                        lax.dot_general(
+                            part,
+                            ret[place, :, start : start + chunk],
+                            (((0,), (0,)), ((), ())),
+                            preferred_element_type=jnp.float32,
+                        )
+                        for part in splits[lane]
                     )
-                    for part in (high, low)
-                )
-
-                @pl.when(core == lane)
-                def _():
-                    own_half[:, start : start + chunk] = piece
-
-                @pl.when(core != lane)
-                def _():
-                    cross_send[place, :, start : start + chunk] = piece.astype(jnp.bfloat16)
-
-        cross_copy(place).start()
-        cross_copy(place).wait_recv()
-        own_half[...] = own_half[...] + cross[place].astype(jnp.float32)
-
-        @pl.when(jnp.logical_and(z > 0, place >= z))
-        def _():
-            pltpu.make_async_copy(hidden_ref, line_in.at[place], line_recv.at[place]).wait()
-            own_half[...] = own_half[...] + line_in[place].astype(jnp.float32)
-
-        @pl.when(jnp.logical_and(z < n_z - 1, place <= z))
-        def _():
-            spot = jnp.where(place == z, n_z, place)
-            pltpu.make_async_copy(hidden_ref, line_in.at[spot], line_recv.at[spot]).wait()
-            own_half[...] = own_half[...] + line_in[spot].astype(jnp.float32)
+
+                    @pl.when(core == lane)
+                    def _():
+                        own_half[:, start : start + chunk] = piece
+
+                    @pl.when(core != lane)
+                    def _():
+                        cross_send[place, :, start : start + chunk] = piece.astype(jnp.bfloat16)
+
+            cross_copy(place, h).start()
+
+        for h in range(parts):
+            cols = columns(h)
+            cross_copy(place, h).wait_recv()
+            own_half[:, cols] = own_half[:, cols] + cross[place, :, cols].astype(jnp.float32)
+
+            def add_line(spot):
+                pltpu.make_async_copy(
+                    cross.at[place, :, cols], line_in.at[spot, :, cols], line_recv.at[h, spot]
+                ).wait()
+                own_half[:, cols] = own_half[:, cols] + line_in[spot, :, cols].astype(jnp.float32)
+
+            @pl.when(jnp.logical_and(z > 0, place >= z))
+            def _():
+                add_line(place)
+
+            @pl.when(jnp.logical_and(z < n_z - 1, place <= z))
+            def _():
+                add_line(jnp.where(place == z, n_z, place))
+
+            @pl.when(place > z)
+            def _():
+                cross[place, :, cols] = own_half[:, cols].astype(jnp.bfloat16)
+                sum_copy(place, 0, h).start()
+
+            @pl.when(place < z)
+            def _():
+                cross[place, :, cols] = own_half[:, cols].astype(jnp.bfloat16)
+                sum_copy(place, 1, h).start()
 
         @pl.when(place == z)
         def _():
@@ -1177,21 +1216,17 @@
                 shifted * lax.rsqrt(variance + EPS_LAYER) * norm_gain[...] + norm_bias[...]
             ).astype(jnp.bfloat16)
 
-        @pl.when(place > z)
-        def _():
-            cross[place] = own_half[...].astype(jnp.bfloat16)
-            line_up(place).start()
-
-        @pl.when(place < z)
-        def _():
-            cross[place] = own_half[...].astype(jnp.bfloat16)
-            line_dn(place).start()
+    @pl.loop(0, n_z)
+    def _(step):
+        return_step(step)
 
     @pl.loop(0, n_z + 1)
     def _(step):
-        @pl.when(step < n_z)
-        def _():
-            return_step(step)
+        if by_line:
+
+            @pl.when(jnp.logical_and(relays, step < n_z))
+            def _():
+                far_step(step)
 
         @pl.when(step > 0)
         def _():
@@ -1203,18 +1238,21 @@
 
         @pl.when(jnp.logical_and(place <= z, z < n_z - 1))
         def _():
-            line_copy(hidden_ref, 0, place).wait_send()
+            for h in range(cuts):
+                line_copy(hidden_ref, 0, place, h).wait_send()
 
         @pl.when(jnp.logical_and(place >= z, z > 0))
         def _():
-            line_copy(hidden_ref, 1, place).wait_send()
+            for h in range(cuts):
+                line_copy(hidden_ref, 1, place, h).wait_send()
 
         part_copy(place).wait_send()
-        cross_copy(place).wait_send()
-
-        @pl.when(place != z)
-        def _():
-            line_up(place).wait_send()
+        for h in range(parts):
+            cross_copy(place, h).wait_send()
+
+            @pl.when(place != z)
+            def _():
+                sum_copy(place, 0, h).wait_send()
 
         @pl.loop(1, n_sp)
         def _(j):
@@ -1254,6 +1292,8 @@
     by_line = n_sp == 4
     dma = pltpu.SemaphoreType.DMA
     bf16 = jnp.bfloat16
+    parts = 4
+    cuts = 2
     return pl.pallas_call(
         functools.partial(
             moe_kernel, n_sp=n_sp, tp_size=tp_size, cap=cap, slots=slots, by_line=by_line
@@ -1284,8 +1324,8 @@
             pltpu.VMEM((n_z + 1, slots, width) if by_line else (1, 16, 128), bf16),
             pltpu.VMEM((slots, width) if by_line else (8, 128), jnp.float32),
             dma((6,)),
-            dma((2, n_z)),
-            dma((n_z,)),
+            dma((2 * cuts, n_z)),
+            dma((cuts, n_z)),
             dma((n_z,)),
             dma((n_z,)),
             dma((tp_size,)),
@@ -1298,10 +1338,10 @@
             dma((n_z,)),
             dma((n_z, n_sp)),
             dma((n_z, n_sp)),
-            dma((n_z,)),
-            dma((n_z,)),
-            dma((n_z,)),
-            dma((n_z + 1,)),
+            dma((parts, n_z)),
+            dma((parts, n_z)),
+            dma((parts, n_z)),
+            dma((parts, n_z + 1)),
             dma((2, n_z)),
             dma((n_z,)),
             dma((n_z + 1,)),

time: 207 us -> 197 us (0.952)
  Pallas kernels: 202 us -> 192 us
    pallas_call x1, Pallas kernels: 141 us -> 132 us  [moe(): pl.pallas_call(functools.partial(moe_kernel, n_sp=n_sp, tp_size=tp_size,...]
where the time goes in v2:
time: 197 us; the launch traced here: 196 us
  Pallas kernels  192 us (97%)
    pallas_call x1, Pallas kernels, moe(): pl.pallas_call(functools.partial(moe_kernel, n_sp=n_sp, tp_size=tp_size,...  132 us
    pallas_call x1, Pallas kernels, attention(): pl.pallas_call(functools.partial(attention_kernel, tp_size=tp_size, shard...  60.6 us

profile of v2, /device:TPU:11, one launch (start us, length us, event | category | flops | bytes accessed | tf_op | source)
XLA Modules:
  0.0 196.1 jit_solution(2059293392253641299)
XLA Ops:
  0.0 0.7 convert_element_type.3
  0.7 1.3 maximum_bitcast_fusion.meta_ref
  1.9 60.6 %shard_map.307.hidden_ref = bf16[128,2048]{1,0:T(8,128)(2,1)} custom-call(bf16[1024,128]{1,0:T(8,128)(2,1)} %wide_query.1, bf16[1024,128]{1,0:T(8,128)(2,1)} %narrow_query.1, bf16[1024,256]{1,0:T(8,128)(2,1)} %wide_keys.1, bf16[1024,256]{1,0:T(8,128)(2,1)} %narrow_keys.1, bf16[1024,256]{1,0:T(8,128)(2,1)} %wide_values.1, bf16[1024,256]{1,0:T(8,128)(2,1)} %narrow_values.1, ...), custom_call_target="tpu_custom_call" | custom-call | tf_op jit(solution)/shard_map/pallas_call | solution.py:548
  62.6 131.6 %shard_map.308 = bf16[128,2048]{1,0:T(8,128)(2,1)} custom-call(bf16[128,2048]{1,0:T(8,128)(2,1)} %shard_map.307.hidden_ref, f32[4,128]{1,0:T(4,128)} %maximum_bitcast_fusion.meta_ref, f32[1,2048]{1,0:T(1,128)} %bitcast.12, f32[1,2048]{1,0:T(1,128)} %bitcast.13, bf16[2048,256]{1,0:T(8,128)(2,1)} %shared_gate_hbm.1, bf16[2048,256]{1,0:T(8,128)(2,1)} %shared_up_hbm.1, ...), custom_call_target="tpu_custom_call" | custom-call | tf_op jit(solution)/shard_map/pallas_call | solution.py:1297
  194.2 1.9 copy.35
